TPU v7x, 32 devices: a whole 2x2x4 slice. The times are simulated.
32 devices in a mesh: rep: 2 (over x), fs: 8 (over z, y), tp: 2 (over core).
Axes of the slice: x: 2, y: 2, z: 4, core: 2. Of those that a mesh axis runs over, the one named last changes fastest.
Arguments:
- tokens: bfloat16 [10240, 2048], P(('rep', 'fs'), 'tp'), may hold values from -6 to 6
- norm_first: float32 [2048], replicated, may hold values from 0.1 to 1.9
- norm_mix: float32 [2048], replicated, may hold values from 0.1 to 1.9
- norm_second: float32 [2048], replicated, may hold values from 0.1 to 1.9
- gate_weight: float32 [2048, 2816], P('fs', 'tp'), may hold values from -0.125 to 0.125
- up_weight: float32 [2048, 2816], P('fs', 'tp'), may hold values from -0.125 to 0.125
- down_weight: float32 [2816, 2048], P('tp', 'fs'), may hold values from -0.109375 to 0.109375
- gate_scale: float32 [2816], P('tp'), may hold values from 0.3 to 3
- up_scale: float32 [2816], P('tp'), may hold values from 0.3 to 3
- down_scale: float32 [2048], P('fs'), may hold values from 0.3 to 3
- u_weight: float32 [2048, 1024], P('fs', 'tp'), may hold values from -0.125 to 0.125
- v_weight: float32 [2048, 1024], P('fs', 'tp'), may hold values from -0.125 to 0.125
- u_scale: float32 [1024], P('tp'), may hold values from 0.3 to 3
- v_scale: float32 [1024], P('tp'), may hold values from 0.15 to 6
- ln_gain: float32 [1024], P('tp'), may hold values from 0.1 to 1.9
- ln_bias: float32 [1024], P('tp'), may hold values from -3 to 3
- spatial_weight: bfloat16 [8, 128, 128], P('tp'), may hold values from -0.25 to 0.25
- spatial_bias: float32 [8, 128], P('tp'), may hold values from 0.1 to 1.9
- out_weight: float32 [1024, 2048], P('tp', 'fs'), may hold values from -0.1875 to 0.1875
- out_scale: float32 [2048], P('fs'), may hold values from 0.3 to 3
Outputs:
- layer_out: bfloat16 [10240, 2048], P(('rep', 'fs'), 'tp')
All inputs are finite; a program needn't handle non-finite values.
Results may differ from a plain program's by a relative error of at most 0.019.
Values may be sent and summed in bfloat16 or wider, within the bound.
No kernel may reach another device: no remote copies, remote signals or barrier semaphores. Data moves between devices by JAX's collectives and lax.ppermute only.
A program may use at most 128 MiB of HBM per device.

v0:
```python
import jax
import jax.numpy as jnp
from jax import lax
from jax.sharding import PartitionSpec as P

BW = 1024
SPAN = 128
EPS = 1e-06


def add_pair(left, pieces):
    return (
        jnp.dot(left, pieces[0], preferred_element_type=jnp.float32),
        jnp.dot(left, pieces[1], preferred_element_type=jnp.float32),
    )


def on_device(
    tokens,
    norm_first,
    norm_mix,
    norm_second,
    gate_weight,
    up_weight,
    down_weight,
    gate_scale,
    up_scale,
    down_scale,
    u_weight,
    v_weight,
    u_scale,
    v_scale,
    ln_gain,
    ln_bias,
    spatial_weight,
    spatial_bias,
    out_weight,
    out_scale,
):
    wide_scales = (
        lax.all_gather(down_scale, "fs", axis=0, tiled=True),
        lax.all_gather(out_scale, "fs", axis=0, tiled=True),
    )
    gate_low = gate_weight.astype(jnp.bfloat16)
    up_low = up_weight.astype(jnp.bfloat16)
    down_low = down_weight.astype(jnp.bfloat16)
    count = tokens.shape[0]

    def full_norm(rows, gain):
        whole = lax.all_gather(rows, "tp", axis=1, tiled=True)
        values = whole.astype(jnp.float32)
        factor = lax.rsqrt(jnp.mean(values * values, axis=1, keepdims=True) + EPS)
        return (values * factor * gain).astype(jnp.bfloat16)

    def spread_sum(term):
        return lax.psum_scatter(
            term.astype(jnp.bfloat16), "tp", scatter_dimension=1, tiled=True
        ).astype(jnp.float32)

    gate_all, up_all = (
        lax.all_gather(gate_low, "fs", axis=0, tiled=True),
        lax.all_gather(up_low, "fs", axis=0, tiled=True),
    )

    def hidden_units(normed):
        gate = jnp.dot(normed, gate_all, preferred_element_type=jnp.float32) * gate_scale
        up_part = jnp.dot(normed, up_all, preferred_element_type=jnp.float32) * up_scale
        return (jax.nn.silu(gate) * up_part).astype(jnp.bfloat16)

    first_hidden = hidden_units(full_norm(tokens, norm_first))
    down_all = lax.all_gather(down_low, "fs", axis=1, tiled=True)
    first_term = (
        jnp.dot(first_hidden, down_all, preferred_element_type=jnp.float32) * wide_scales[0]
    )
    first = spread_sum(first_term)
    middle = (tokens.astype(jnp.float32) + 0.5 * first).astype(jnp.bfloat16)
    mix_normed = full_norm(middle, norm_mix)
    u_low = u_weight.astype(jnp.bfloat16)
    v_low = v_weight.astype(jnp.bfloat16)
    u_acc, v_acc = add_pair(
        mix_normed,
        (
            lax.all_gather(u_low, "fs", axis=0, tiled=True),
            lax.all_gather(v_low, "fs", axis=0, tiled=True),
        ),
    )
    u_pre = u_acc * u_scale
    v_act = jax.nn.gelu(v_acc * v_scale, approximate=True)
    totals = lax.psum((jnp.sum(v_act, axis=1), jnp.sum(v_act * v_act, axis=1)), "tp")
    v_mean = (totals[0] / BW)[:, None]
    v_var = (totals[1] / BW)[:, None] - v_mean * v_mean
    v_normed = ((v_act - v_mean) * lax.rsqrt(v_var + EPS) * ln_gain + ln_bias).astype(jnp.bfloat16)
    local_groups = spatial_weight.shape[0]
    channels = v_act.shape[1] // local_groups
    blocks = v_normed.reshape(count // SPAN, SPAN, local_groups, channels)
    lower = jnp.tril(jnp.ones((SPAN, SPAN), jnp.bool_))
    masked = jnp.where(lower[None], spatial_weight, jnp.zeros_like(spatial_weight))
    spatial = jnp.einsum("gts,nsgc->ntgc", masked, blocks, preferred_element_type=jnp.float32)
    spatial = spatial + spatial_bias.T[None, :, :, None]
    mixed = (jax.nn.gelu(u_pre, approximate=True) * spatial.reshape(count, v_act.shape[1])).astype(
        jnp.bfloat16
    )
    out_low = out_weight.astype(jnp.bfloat16)
    mix_term = (
        jnp.dot(
            mixed,
            lax.all_gather(out_low, "fs", axis=1, tiled=True),
            preferred_element_type=jnp.float32,
        )
        * wide_scales[1]
    )
    second = (middle.astype(jnp.float32) + spread_sum(mix_term)).astype(jnp.bfloat16)
    second_hidden = hidden_units(full_norm(second, norm_second))
    last = spread_sum(
        jnp.dot(second_hidden, down_all, preferred_element_type=jnp.float32) * wide_scales[0]
    )
    return (second.astype(jnp.float32) + 0.5 * last).astype(jnp.bfloat16)


def solution(mesh):
    placed = (
        P(("rep", "fs"), "tp"),
        P(),
        P(),
        P(),
        P("fs", "tp"),
        P("fs", "tp"),
        P("tp", "fs"),
        P("tp"),
        P("tp"),
        P("fs"),
        P("fs", "tp"),
        P("fs", "tp"),
        P("tp"),
        P("tp"),
        P("tp"),
        P("tp"),
        P("tp", None, None),
        P("tp", None),
        P("tp", "fs"),
        P("fs"),
    )
    return jax.shard_map(
        on_device, mesh=mesh, in_specs=placed, out_specs=P(("rep", "fs"), "tp"), check_vma=False
    )
```

profile of v0, /device:TPU:0, one launch (start us, length us, event | category | flops | bytes accessed | tf_op | source)
XLA Modules:
  0.0 577.7 jit_solution(11312762153509955955)
XLA Ops:
  7.3 2.4 convert_element_type.87
  9.8 0.9 convert_element_type.88
  10.9 0.9 convert_element_type.90
  11.9 22.3 %all-gather = f32[8,1,256]{2,1,0:T(1,128)S(1)} all-gather(f32[1,1,256]{2,1,0:T(1,128)S(1)} %bitcast.34), channel_id=1, replica_groups=mesh['rep'=2,'fs'=8,'tp'=2] {'fs'}, dimensions={0}, use_global_device_ids=true | all-gather | bytes 9216 | tf_op jit(solution)/shard_map/all_gather | solution.py:41
  34.2 2.6 fusion
  36.9 81.8 %all-gather.14.cloned.1.call-done = bf16[2048,1408]{1,0:T(8,128)(2,1)} async-done(((bf16[256,1408]{1,0:T(8,128)(2,1)}), bf16[2048,1408]{1,0:T(8,128)(2,1)}) %all-gather.14.cloned.1.call-update) | async-done | bytes 5767184 | tf_op jit(solution)/shard_map/all_gather | solution.py:61
  118.7 8.7 %convolution_multiply_fusion.3 = f32[640,1408]{1,0:T(8,128)} fusion(bf16[2048,1408]{1,0:T(8,128)(2,1)} %all-gather.14.cloned.1.call-done, f32[1408]{0:T(1024)S(1)} %copy-done.19, bf16[640,2048]{1,0:T(8,128)(2,1)S(1)} %copy-done.4, f32[2048]{0:T(1024)S(1)} %copy-done.17, f32[640]{0:T(1024)S(1)} %add_rsqrt_fusion.3), kind=kOutput, calls=%fused_computation.23 | convolution fusion | flops 3697131520 | bytes 12009472 | tf_op jit(solution)/shard_map/dot_general | solution.py:66
  127.4 84.0 %all-gather.16.cloned.1.call-done = bf16[2048,1408]{1,0:T(8,128)(2,1)} async-done(((bf16[256,1408]{1,0:T(8,128)(2,1)}), bf16[2048,1408]{1,0:T(8,128)(2,1)}) %all-gather.16.cloned.1.call-update) | async-done | bytes 5767184 | tf_op jit(solution)/shard_map/all_gather | solution.py:62
  211.4 93.2 %all-gather.18.cloned.1.call-done = bf16[1408,2048]{1,0:T(8,128)(2,1)} async-done(((bf16[1408,256]{1,0:T(8,128)(2,1)}), bf16[1408,2048]{1,0:T(8,128)(2,1)}) %all-gather.18.cloned.1.call-update) | async-done | bytes 5767184 | tf_op jit(solution)/shard_map/all_gather | solution.py:71
  304.6 15.4 %multiply_convert_fusion.2 = bf16[640,2048]{1,0:T(8,128)(2,1)} fusion(bf16[1408,2048]{1,0:T(8,128)(2,1)} %all-gather.18.cloned.1.call-done, f32[2048]{0:T(1024)S(1)} %bitcast.30, bf16[2048,1408]{1,0:T(8,128)(2,1)} %all-gather.16.cloned.1.call-done, f32[640,1408]{1,0:T(8,128)} %convolution_multiply_fusion.3, f32[1408]{0:T(1024)S(1)} %copy-done.20, ...), kind=kOutput, calls=%fused_computation.17 | convolution fusion | flops 7396147200 | bytes 20406272 | tf_op jit(solution)/shard_map/dot_general | solution.py:73
  320.1 8.5 %reduce-scatter.4.cloned.1.call-done = bf16[640,1024]{1,0:T(8,128)(2,1)} async-done(((bf16[640,2048]{1,0:T(8,128)(2,1)}), bf16[640,1024]{1,0:T(8,128)(2,1)}) %reduce-scatter.4.cloned.1.call-update) | async-done | bytes 1310736 | tf_op jit(solution)/shard_map/reduce_scatter | solution.py:56
  328.7 2.9 add_convert_fusion.2
  331.7 0.7 convert_element_type.98
  332.5 0.7 convert_element_type.97
  334.2 21.1 %all-gather.1 = f32[8,1,256]{2,1,0:T(1,128)S(1)} all-gather(f32[1,1,256]{2,1,0:T(1,128)S(1)} %bitcast.35), channel_id=1, replica_groups=mesh['rep'=2,'fs'=8,'tp'=2] {'fs'}, dimensions={0}, use_global_device_ids=true | all-gather | bytes 9216 | tf_op jit(solution)/shard_map/all_gather | solution.py:42
  355.3 2.6 fusion.3
  357.9 38.9 %all-gather.24.cloned.1.call-done = bf16[2048,512]{1,0:T(8,128)(2,1)} async-done(((bf16[256,512]{1,0:T(8,128)(2,1)}), bf16[2048,512]{1,0:T(8,128)(2,1)}) %all-gather.24.cloned.1.call-update) | async-done | bytes 2097168 | tf_op jit(solution)/shard_map/all_gather | solution.py:84
  396.8 4.6 fusion.57
  401.4 2.6 all-reduce
  404.1 1.6 add_convert_fusion.3
  406.3 1.0 copy.26
  407.3 39.3 %all-gather.22.cloned.1.call-done = bf16[2048,512]{1,0:T(8,128)(2,1)} async-done(((bf16[256,512]{1,0:T(8,128)(2,1)}), bf16[2048,512]{1,0:T(8,128)(2,1)}) %all-gather.22.cloned.1.call-update) | async-done | bytes 2097168 | tf_op jit(solution)/shard_map/all_gather | solution.py:83
  446.6 51.0 %all-gather.26.cloned.1.call-done = bf16[512,2048]{1,0:T(8,128)(2,1)} async-done(((bf16[512,256]{1,0:T(8,128)(2,1)}), bf16[512,2048]{1,0:T(8,128)(2,1)}) %all-gather.26.cloned.1.call-update) | async-done | bytes 2097168 | tf_op jit(solution)/shard_map/all_gather | solution.py:107
  497.6 7.8 %multiply_convert_fusion.1 = bf16[640,2048]{1,0:T(8,128)(2,1)} fusion(bf16[512,2048]{1,0:T(8,128)(2,1)} %all-gather.26.cloned.1.call-done, f32[2048]{0:T(1024)S(1)} %bitcast.32, f32[80,8,4,128]{3,2,1,0:T(4,128)S(1)} %bitcast.29, bf16[2048,512]{1,0:T(8,128)(2,1)} %all-gather.22.cloned.1.call-done, bf16[640,2048]{1,0:T(8,128)(2,1)} %all-gather.20.cloned.1.call-done, ...), kind=kOutput, calls=%fused_computation.16 | convolution fusion | flops 2695823360 | bytes 10768896 | tf_op jit(solution)/shard_map/dot_general | solution.py:105
  505.4 8.6 %reduce-scatter.6.cloned.1.call-done = bf16[640,1024]{1,0:T(8,128)(2,1)} async-done(((bf16[640,2048]{1,0:T(8,128)(2,1)}), bf16[640,1024]{1,0:T(8,128)(2,1)}) %reduce-scatter.6.cloned.1.call-update) | async-done | bytes 1310736 | tf_op jit(solution)/shard_map/reduce_scatter | solution.py:56
  514.0 2.9 add_convert_fusion.1
  517.2 12.5 %all-gather.28.cloned.1.call-done = bf16[640,2048]{1,0:T(8,128)(2,1)} async-done(((bf16[640,1024]{1,0:T(8,128)(2,1)}), bf16[640,2048]{1,0:T(8,128)(2,1)}) %all-gather.28.cloned.1.call-update) | async-done | bytes 2621456 | tf_op jit(solution)/shard_map/all_gather | solution.py:50
  529.7 2.5 fusion.6
  532.2 8.7 %convolution_multiply_fusion.1 = f32[640,1408]{1,0:T(8,128)} fusion(bf16[2048,1408]{1,0:T(8,128)(2,1)} %all-gather.14.cloned.1.call-done, f32[1408]{0:T(1024)S(1)} %copy-done.19, bf16[640,2048]{1,0:T(8,128)(2,1)S(1)} %copy-done.5, f32[2048]{0:T(1024)S(1)} %copy-done.21, f32[640]{0:T(1024)S(1)} %add_rsqrt_fusion), kind=kOutput, calls=%fused_computation.20 | convolution fusion | flops 3697131520 | bytes 12009472 | tf_op jit(solution)/shard_map/dot_general | solution.py:66
  540.9 15.4 %multiply_convert_fusion = bf16[640,2048]{1,0:T(8,128)(2,1)} fusion(bf16[1408,2048]{1,0:T(8,128)(2,1)} %all-gather.18.cloned.1.call-done, f32[2048]{0:T(1024)S(1)} %bitcast.31, bf16[2048,1408]{1,0:T(8,128)(2,1)} %all-gather.16.cloned.1.call-done, f32[640,1408]{1,0:T(8,128)} %convolution_multiply_fusion.1, f32[1408]{0:T(1024)S(1)} %copy-done.20, ...), kind=kOutput, calls=%fused_computation.15 | convolution fusion | flops 7396147200 | bytes 20406272 | tf_op jit(solution)/shard_map/dot_general | solution.py:115
  556.3 11.6 %reduce-scatter.8.cloned.1.call-done = bf16[640,1024]{1,0:T(8,128)(2,1)} async-done(((bf16[640,2048]{1,0:T(8,128)(2,1)}), bf16[640,1024]{1,0:T(8,128)(2,1)}) %reduce-scatter.8.cloned.1.call-update) | async-done | bytes 1310736 | tf_op jit(solution)/shard_map/reduce_scatter | solution.py:56
  567.9 2.9 add_convert_fusion
  (82 shorter events, 3.1 us)
Async XLA Ops:
  6.5 3.3 copy-start.6
  6.5 27.7 %all-gather.12.cloned.1.call-start = ((), (), s32[]{:S(2)}) async-start(), calls=%async_computation.3 | async-start | bytes 3932160 | tf_op jit(solution)/shard_map/all_gather | solution.py:50
  7.3 3.6 copy-start.7
  7.3 111.4 %all-gather.14.cloned.1.call-start = ((), (), s32[]{:S(2)}) async-start(), calls=%async_computation.4 | async-start | bytes 6488064 | tf_op jit(solution)/shard_map/all_gather | solution.py:61
  9.8 201.6 %all-gather.16.cloned.1.call-start = ((), (), s32[]{:S(2)}) async-start(), calls=%async_computation.5 | async-start | bytes 6488064 | tf_op jit(solution)/shard_map/all_gather | solution.py:62
  10.8 107.9 %copy-start.17 = (f32[2048]{0:T(1024)S(1)}, f32[2048]{0:T(1024)}, u32[]{:S(2)}) copy-start(f32[2048]{0:T(1024)} %param.21) | copy-start | bytes 24580
  10.8 107.9 %copy-start.19 = (f32[1408]{0:T(1024)S(1)}, f32[1408]{0:T(1024)}, u32[]{:S(2)}) copy-start(f32[1408]{0:T(1024)} %param.27) | copy-start | bytes 16900
  10.8 293.8 %all-gather.18.cloned.1.call-start = ((), (), s32[]{:S(2)}) async-start(), calls=%async_computation.6 | async-start | bytes 6488064 | tf_op jit(solution)/shard_map/all_gather | solution.py:71
  11.8 316.8 %reduce-scatter.4.cloned.1.call-start = ((), (), s32[]{:S(2)}) async-start(), calls=%async_computation.7 | async-start | bytes 3932160 | tf_op jit(solution)/shard_map/reduce_scatter | solution.py:56
  34.2 84.5 %copy-start.4 = (bf16[640,2048]{1,0:T(8,128)(2,1)S(1)}, bf16[640,2048]{1,0:T(8,128)(2,1)}, u32[]{:S(2)}) copy-start(bf16[640,2048]{1,0:T(8,128)(2,1)} %all-gather.12.cloned.1.call-done) | copy-start | bytes 7864324
  36.9 267.8 %copy-start.20 = (f32[1408]{0:T(1024)S(1)}, f32[1408]{0:T(1024)}, u32[]{:S(2)}) copy-start(f32[1408]{0:T(1024)} %param.28) | copy-start | bytes 16900
  320.0 8.7 %copy-start.2 = (bf16[640,1024]{1,0:T(8,128)(2,1)S(1)}, bf16[640,1024]{1,0:T(8,128)(2,1)}, u32[]{:S(2)}) copy-start(bf16[640,1024]{1,0:T(8,128)(2,1)} %param.20) | copy-start | bytes 3932164
  320.1 11.6 %copy-start.8 = (f32[256,512]{1,0:T(8,128)S(1)}, f32[256,512]{1,0:T(8,128)}, u32[]{:S(2)}) copy-start(f32[256,512]{1,0:T(8,128)} %param.31) | copy-start | bytes 1572868
  320.1 12.5 %copy-start.9 = (f32[256,512]{1,0:T(8,128)S(1)}, f32[256,512]{1,0:T(8,128)}, u32[]{:S(2)}) copy-start(f32[256,512]{1,0:T(8,128)} %param.30) | copy-start | bytes 1572868
  320.1 35.2 %all-gather.20.cloned.1.call-start = ((), (), s32[]{:S(2)}) async-start(), calls=%async_computation.8 | async-start | bytes 3932160 | tf_op jit(solution)/shard_map/all_gather | solution.py:50
  331.6 65.2 %all-gather.24.cloned.1.call-start = ((), (), s32[]{:S(2)}) async-start(), calls=%async_computation.10 | async-start | bytes 2359296 | tf_op jit(solution)/shard_map/all_gather | solution.py:84
  332.4 64.4 %copy-start.18 = (f32[2048]{0:T(1024)S(1)}, f32[2048]{0:T(1024)}, u32[]{:S(2)}) copy-start(f32[2048]{0:T(1024)} %param.22) | copy-start | bytes 24580
  332.4 64.4 %copy-start.22 = (f32[512]{0:T(512)S(1)}, f32[512]{0:T(512)}, u32[]{:S(2)}) copy-start(f32[512]{0:T(512)} %param.33) | copy-start | bytes 6148
  332.5 114.1 %all-gather.22.cloned.1.call-start = ((), (), s32[]{:S(2)}) async-start(), calls=%async_computation.9 | async-start | bytes 2359296 | tf_op jit(solution)/shard_map/all_gather | solution.py:83
  333.3 164.3 %all-gather.26.cloned.1.call-start = ((), (), s32[]{:S(2)}) async-start(), calls=%async_computation.11 | async-start | bytes 2359296 | tf_op jit(solution)/shard_map/all_gather | solution.py:107
  334.1 179.9 %reduce-scatter.6.cloned.1.call-start = ((), (), s32[]{:S(2)}) async-start(), calls=%async_computation.12 | async-start | bytes 3932160 | tf_op jit(solution)/shard_map/reduce_scatter | solution.py:56
  355.3 41.5 %copy-start.3 = (bf16[640,2048]{1,0:T(8,128)(2,1)S(1)}, bf16[640,2048]{1,0:T(8,128)(2,1)}, u32[]{:S(2)}) copy-start(bf16[640,2048]{1,0:T(8,128)(2,1)} %all-gather.20.cloned.1.call-done) | copy-start | bytes 7864324
  357.9 46.2 %copy-start.13 = (f32[512]{0:T(512)S(1)}, f32[512]{0:T(512)}, u32[]{:S(2)}) copy-start(f32[512]{0:T(512)} %param.35) | copy-start | bytes 6148
  357.9 46.2 %copy-start.14 = (f32[512]{0:T(512)S(1)}, f32[512]{0:T(512)}, u32[]{:S(2)}) copy-start(f32[512]{0:T(512)} %param.34) | copy-start | bytes 6148
  401.4 4.4 copy-start.11
  401.4 4.5 copy-start.12
  405.9 91.7 %copy-start.23 = (f32[512]{0:T(512)S(1)}, f32[512]{0:T(512)}, u32[]{:S(2)}) copy-start(f32[512]{0:T(512)} %param.32) | copy-start | bytes 6148
  505.3 8.7 %copy-start = (bf16[640,1024]{1,0:T(8,128)(2,1)S(1)}, bf16[640,1024]{1,0:T(8,128)(2,1)}, u32[]{:S(2)}) copy-start(bf16[640,1024]{1,0:T(8,128)(2,1)} %add_convert_fusion.2) | copy-start | bytes 3932164
  505.4 24.4 %all-gather.28.cloned.1.call-start = ((), (), s32[]{:S(2)}) async-start(), calls=%async_computation.13 | async-start | bytes 3932160 | tf_op jit(solution)/shard_map/all_gather | solution.py:50
  516.9 15.3 %copy-start.21 = (f32[2048]{0:T(1024)S(1)}, f32[2048]{0:T(1024)}, u32[]{:S(2)}) copy-start(f32[2048]{0:T(1024)} %param.23) | copy-start | bytes 24580
  516.9 51.0 %reduce-scatter.8.cloned.1.call-start = ((), (), s32[]{:S(2)}) async-start(), calls=%async_computation.14 | async-start | bytes 3932160 | tf_op jit(solution)/shard_map/reduce_scatter | solution.py:56
  556.3 11.6 %copy-start.1 = (bf16[640,1024]{1,0:T(8,128)(2,1)S(1)}, bf16[640,1024]{1,0:T(8,128)(2,1)}, u32[]{:S(2)}) copy-start(bf16[640,1024]{1,0:T(8,128)(2,1)} %add_convert_fusion.1) | copy-start | bytes 3932164
  (4 other events, 8.9 us)
Sparse Core Ops, SparseCore 0:
  8.9 14.0 all-gather.11
  25.2 93.4 all-gather.13
  120.9 90.4 all-gather.15
  213.3 91.2 all-gather.17
  320.2 8.4 reduce-scatter.3
  331.8 12.6 all-gather.19
  346.5 50.2 all-gather.23
  399.0 47.6 all-gather.21
  448.7 48.8 all-gather.25
  505.5 8.4 reduce-scatter.5
  517.0 12.6 all-gather.27
  556.4 11.4 reduce-scatter.7
where the time goes:
time: 578 us
  waiting for transfers between devices  430 us (74%)
  matrix products  60.8 us (11%)
  blocking collectives  46 us (8%)
  other arithmetic  24.6 us (4%)
  between operations  13.8 us (2%)
    all_gather x1, waiting for transfers between devices, on_device(): down_all = lax.all_gather(down_low, 'fs', axis=1, tiled=True)  93.2 us
    all_gather x1, waiting for transfers between devices, on_device(): lax.all_gather(up_low, 'fs', axis=0, tiled=True)  84 us
    all_gather x1, waiting for transfers between devices, on_device(): lax.all_gather(gate_low, 'fs', axis=0, tiled=True)  81.8 us
    all_gather x1, waiting for transfers between devices, on_device(): lax.all_gather(out_low, 'fs', axis=1, tiled=True)  51 us
    all_gather x1, waiting for transfers between devices, on_device(): lax.all_gather(u_low, 'fs', axis=0, tiled=True)  39.3 us
    all_gather x1, waiting for transfers between devices, on_device(): lax.all_gather(v_low, 'fs', axis=0, tiled=True)  38.9 us
    reduce_scatter x3, waiting for transfers between devices, spread_sum(): lax.psum_scatter(term.astype(jnp.bfloat16), 'tp', scatter_dimension=1, ti...  28.7 us
    all_gather x1, blocking collectives, on_device(): lax.all_gather(down_scale, 'fs', axis=0, tiled=True)  22.3 us
  transfers between devices with their start and end apart: 12, of which 10 were waited for; matrix products, arithmetic and copies ran while one was open for 5% of the time, Pallas kernels for 0%

commit v1 on v0

--- a/solution.py
+++ b/solution.py
@@ -104,7 +104,7 @@
     mix_term = (
         jnp.dot(
             mixed,
-            lax.all_gather(out_low, "fs", axis=1, tiled=True),
+            jnp.concatenate(lax.all_gather(out_low, "fs"), axis=1),
             preferred_element_type=jnp.float32,
         )
         * wide_scales[1]

time: 578 us -> 576 us (level)
  waiting for transfers between devices: 430 us -> 423 us
    all_gather x1, waiting for transfers between devices: 51 us -> 26.7 us  [on_device(): lax.all_gather(out_low, 'fs')]
    all_gather x1, waiting for transfers between devices: 38.9 us -> 49.9 us  [on_device(): lax.all_gather(v_low, 'fs', axis=0, tiled=True)]
    all_gather x3, waiting for transfers between devices: 12.5 us -> 20 us  [full_norm(): whole = lax.all_gather(rows, 'tp', axis=1, tiled=True)]
  transfers between devices with their start and end apart: 12 -> 12, of which waited for: 10 -> 11; matrix products, arithmetic and copies ran while one was open for 5% -> 6% of each run, Pallas kernels for 0% -> 0%
where the time goes in v1:
time: 576 us; the launch traced here: 575 us
  waiting for transfers between devices  423 us (73%)
  matrix products  60.9 us (11%)
  blocking collectives  46 us (8%)
  other arithmetic  24.5 us (4%)
  between operations  13.8 us (2%)
  local copies, waits for them, and re-layouts  6.19 us (1%)
    all_gather x1, waiting for transfers between devices, on_device(): down_all = lax.all_gather(down_low, 'fs', axis=1, tiled=True)  93.2 us
    all_gather x1, waiting for transfers between devices, on_device(): lax.all_gather(up_low, 'fs', axis=0, tiled=True)  84 us
    all_gather x1, waiting for transfers between devices, on_device(): lax.all_gather(gate_low, 'fs', axis=0, tiled=True)  81.8 us
    all_gather x1, waiting for transfers between devices, on_device(): lax.all_gather(v_low, 'fs', axis=0, tiled=True)  49.9 us
    all_gather x1, waiting for transfers between devices, on_device(): lax.all_gather(u_low, 'fs', axis=0, tiled=True)  39.2 us
    reduce_scatter x3, waiting for transfers between devices, spread_sum(): lax.psum_scatter(term.astype(jnp.bfloat16), 'tp', scatter_dimension=1, ti...  27.3 us
    all_gather x1, waiting for transfers between devices, on_device(): lax.all_gather(out_low, 'fs')  26.7 us
    all_gather x1, blocking collectives, on_device(): lax.all_gather(down_scale, 'fs', axis=0, tiled=True)  22.3 us
  transfers between devices with their start and end apart: 12, of which 11 were waited for; matrix products, arithmetic and copies ran while one was open for 6% of the time, Pallas kernels for 0%

profile of v1, /device:TPU:0, one launch (start us, length us, event | category | flops | bytes accessed | tf_op | source)
XLA Modules:
  0.0 575.2 jit_solution(9255359540649770675)
XLA Ops:
  7.3 2.4 convert_element_type.87
  9.8 0.9 convert_element_type.88
  11.9 22.3 %all-gather.1 = f32[8,1,256]{2,1,0:T(1,128)S(1)} all-gather(f32[1,1,256]{2,1,0:T(1,128)S(1)} %bitcast.40), channel_id=1, replica_groups=mesh['rep'=2,'fs'=8,'tp'=2] {'fs'}, dimensions={0}, use_global_device_ids=true | all-gather | bytes 9216 | tf_op jit(solution)/shard_map/all_gather | solution.py:41
  34.2 2.6 fusion
  36.9 81.8 %all-gather.15.cloned.1.call-done = bf16[2048,1408]{1,0:T(8,128)(2,1)} async-done(((bf16[256,1408]{1,0:T(8,128)(2,1)}), bf16[2048,1408]{1,0:T(8,128)(2,1)}) %all-gather.15.cloned.1.call-update) | async-done | bytes 5767184 | tf_op jit(solution)/shard_map/all_gather | solution.py:61
  118.7 8.7 %convolution_multiply_fusion.3 = f32[640,1408]{1,0:T(8,128)} fusion(bf16[2048,1408]{1,0:T(8,128)(2,1)} %all-gather.15.cloned.1.call-done, f32[1408]{0:T(1024)S(1)} %copy-done.19, bf16[640,2048]{1,0:T(8,128)(2,1)S(1)} %copy-done.4, f32[2048]{0:T(1024)S(1)} %copy-done.17, f32[640]{0:T(1024)S(1)} %add_rsqrt_fusion.3), kind=kOutput, calls=%fused_computation.23 | convolution fusion | flops 3697131520 | bytes 12009472 | tf_op jit(solution)/shard_map/dot_general | solution.py:66
  127.4 84.0 %all-gather.17.cloned.1.call-done = bf16[2048,1408]{1,0:T(8,128)(2,1)} async-done(((bf16[256,1408]{1,0:T(8,128)(2,1)}), bf16[2048,1408]{1,0:T(8,128)(2,1)}) %all-gather.17.cloned.1.call-update) | async-done | bytes 5767184 | tf_op jit(solution)/shard_map/all_gather | solution.py:62
  211.4 93.2 %all-gather.19.cloned.1.call-done = bf16[1408,2048]{1,0:T(8,128)(2,1)} async-done(((bf16[1408,256]{1,0:T(8,128)(2,1)}), bf16[1408,2048]{1,0:T(8,128)(2,1)}) %all-gather.19.cloned.1.call-update) | async-done | bytes 5767184 | tf_op jit(solution)/shard_map/all_gather | solution.py:71
  304.6 15.4 %multiply_convert_fusion.2 = bf16[640,2048]{1,0:T(8,128)(2,1)} fusion(bf16[1408,2048]{1,0:T(8,128)(2,1)} %all-gather.19.cloned.1.call-done, f32[2048]{0:T(1024)S(1)} %bitcast.36, bf16[2048,1408]{1,0:T(8,128)(2,1)} %all-gather.17.cloned.1.call-done, f32[640,1408]{1,0:T(8,128)} %convolution_multiply_fusion.3, f32[1408]{0:T(1024)S(1)} %copy-done.20, ...), kind=kOutput, calls=%fused_computation.17 | convolution fusion | flops 7396147200 | bytes 20406272 | tf_op jit(solution)/shard_map/dot_general | solution.py:73
  320.1 1.0 copy-done.8
  321.9 6.8 %reduce-scatter.4.cloned.1.call-done = bf16[640,1024]{1,0:T(8,128)(2,1)} async-done(((bf16[640,2048]{1,0:T(8,128)(2,1)}), bf16[640,1024]{1,0:T(8,128)(2,1)}) %reduce-scatter.4.cloned.1.call-update) | async-done | bytes 1310736 | tf_op jit(solution)/shard_map/reduce_scatter | solution.py:56
  328.7 2.9 add_convert_fusion.2
  333.4 21.1 %all-gather.2 = f32[8,1,256]{2,1,0:T(1,128)S(1)} all-gather(f32[1,1,256]{2,1,0:T(1,128)S(1)} %bitcast.41), channel_id=1, replica_groups=mesh['rep'=2,'fs'=8,'tp'=2] {'fs'}, dimensions={0}, use_global_device_ids=true | all-gather | bytes 9216 | tf_op jit(solution)/shard_map/all_gather | solution.py:42
  354.5 26.7 %all-gather.29.cloned.1.call-done = bf16[4096,256]{1,0:T(8,128)(2,1)} async-done(((bf16[512,256]{1,0:T(8,128)(2,1)}), bf16[4096,256]{1,0:T(8,128)(2,1)}) %all-gather.29.cloned.1.call-update) | async-done | bytes 2097168 | tf_op jit(solution)/shard_map/all_gather | solution.py:107
  381.2 3.9 copy.34
  385.1 7.5 %all-gather.21.cloned.1.call-done = bf16[640,2048]{1,0:T(8,128)(2,1)} async-done(((bf16[640,1024]{1,0:T(8,128)(2,1)}), bf16[640,2048]{1,0:T(8,128)(2,1)}) %all-gather.21.cloned.1.call-update) | async-done | bytes 2621456 | tf_op jit(solution)/shard_map/all_gather | solution.py:50
  392.6 2.5 fusion.3
  395.1 49.9 %all-gather.25.cloned.1.call-done = bf16[2048,512]{1,0:T(8,128)(2,1)} async-done(((bf16[256,512]{1,0:T(8,128)(2,1)}), bf16[2048,512]{1,0:T(8,128)(2,1)}) %all-gather.25.cloned.1.call-update) | async-done | bytes 2097168 | tf_op jit(solution)/shard_map/all_gather | solution.py:84
  445.0 4.7 fusion.57
  449.7 2.6 all-reduce
  452.3 1.6 add_convert_fusion.3
  454.6 1.0 copy.33
  455.6 39.2 %all-gather.23.cloned.1.call-done = bf16[2048,512]{1,0:T(8,128)(2,1)} async-done(((bf16[256,512]{1,0:T(8,128)(2,1)}), bf16[2048,512]{1,0:T(8,128)(2,1)}) %all-gather.23.cloned.1.call-update) | async-done | bytes 2097168 | tf_op jit(solution)/shard_map/all_gather | solution.py:83
  494.8 7.7 %multiply_convert_fusion.1 = bf16[640,2048]{1,0:T(8,128)(2,1)} fusion(bf16[512,2048]{0,1:T(8,128)(2,1)} %bitcast.34, f32[2048]{0:T(1024)S(1)} %bitcast.38, f32[80,8,4,128]{3,2,1,0:T(4,128)S(1)} %bitcast.35, bf16[2048,512]{1,0:T(8,128)(2,1)} %all-gather.23.cloned.1.call-done, bf16[640,2048]{1,0:T(8,128)(2,1)} %all-gather.21.cloned.1.call-done, ...), kind=kOutput, calls=%fused_computation.16 | convolution fusion | flops 2695823360 | bytes 10768896 | tf_op jit(solution)/shard_map/dot_general | solution.py:105
  502.6 8.9 %reduce-scatter.6.cloned.1.call-done = bf16[640,1024]{1,0:T(8,128)(2,1)} async-done(((bf16[640,2048]{1,0:T(8,128)(2,1)}), bf16[640,1024]{1,0:T(8,128)(2,1)}) %reduce-scatter.6.cloned.1.call-update) | async-done | bytes 1310736 | tf_op jit(solution)/shard_map/reduce_scatter | solution.py:56
  511.6 2.9 add_convert_fusion.1
  514.8 12.5 %all-gather.27.cloned.1.call-done = bf16[640,2048]{1,0:T(8,128)(2,1)} async-done(((bf16[640,1024]{1,0:T(8,128)(2,1)}), bf16[640,2048]{1,0:T(8,128)(2,1)}) %all-gather.27.cloned.1.call-update) | async-done | bytes 2621456 | tf_op jit(solution)/shard_map/all_gather | solution.py:50
  527.3 2.5 fusion.6
  529.8 8.7 %convolution_multiply_fusion.1 = f32[640,1408]{1,0:T(8,128)} fusion(bf16[2048,1408]{1,0:T(8,128)(2,1)} %all-gather.15.cloned.1.call-done, f32[1408]{0:T(1024)S(1)} %copy-done.19, bf16[640,2048]{1,0:T(8,128)(2,1)S(1)} %copy-done.5, f32[2048]{0:T(1024)S(1)} %copy-done.21, f32[640]{0:T(1024)S(1)} %add_rsqrt_fusion), kind=kOutput, calls=%fused_computation.20 | convolution fusion | flops 3697131520 | bytes 12009472 | tf_op jit(solution)/shard_map/dot_general | solution.py:66
  538.4 15.4 %multiply_convert_fusion = bf16[640,2048]{1,0:T(8,128)(2,1)} fusion(bf16[1408,2048]{1,0:T(8,128)(2,1)} %all-gather.19.cloned.1.call-done, f32[2048]{0:T(1024)S(1)} %bitcast.37, bf16[2048,1408]{1,0:T(8,128)(2,1)} %all-gather.17.cloned.1.call-done, f32[640,1408]{1,0:T(8,128)} %convolution_multiply_fusion.1, f32[1408]{0:T(1024)S(1)} %copy-done.20, ...), kind=kOutput, calls=%fused_computation.15 | convolution fusion | flops 7396147200 | bytes 20406272 | tf_op jit(solution)/shard_map/dot_general | solution.py:115
  553.8 11.6 %reduce-scatter.8.cloned.1.call-done = bf16[640,1024]{1,0:T(8,128)(2,1)} async-done(((bf16[640,2048]{1,0:T(8,128)(2,1)}), bf16[640,1024]{1,0:T(8,128)(2,1)}) %reduce-scatter.8.cloned.1.call-update) | async-done | bytes 1310736 | tf_op jit(solution)/shard_map/reduce_scatter | solution.py:56
  565.5 2.9 add_convert_fusion
  (83 shorter events, 5.4 us)
Async XLA Ops:
  6.5 3.3 copy-start.6
  6.5 27.7 %all-gather.13.cloned.1.call-start = ((), (), s32[]{:S(2)}) async-start(), calls=%async_computation.3 | async-start | bytes 3932160 | tf_op jit(solution)/shard_map/all_gather | solution.py:50
  7.3 3.6 copy-start.7
  7.3 111.4 %all-gather.15.cloned.1.call-start = ((), (), s32[]{:S(2)}) async-start(), calls=%async_computation.4 | async-start | bytes 6488064 | tf_op jit(solution)/shard_map/all_gather | solution.py:61
  9.8 201.6 %all-gather.17.cloned.1.call-start = ((), (), s32[]{:S(2)}) async-start(), calls=%async_computation.5 | async-start | bytes 6488064 | tf_op jit(solution)/shard_map/all_gather | solution.py:62
  10.8 107.9 %copy-start.17 = (f32[2048]{0:T(1024)S(1)}, f32[2048]{0:T(1024)}, u32[]{:S(2)}) copy-start(f32[2048]{0:T(1024)} %param.21) | copy-start | bytes 24580
  10.8 107.9 %copy-start.19 = (f32[1408]{0:T(1024)S(1)}, f32[1408]{0:T(1024)}, u32[]{:S(2)}) copy-start(f32[1408]{0:T(1024)} %param.27) | copy-start | bytes 16900
  10.8 293.8 %all-gather.19.cloned.1.call-start = ((), (), s32[]{:S(2)}) async-start(), calls=%async_computation.6 | async-start | bytes 6488064 | tf_op jit(solution)/shard_map/all_gather | solution.py:71
  11.8 316.8 %reduce-scatter.4.cloned.1.call-start = ((), (), s32[]{:S(2)}) async-start(), calls=%async_computation.7 | async-start | bytes 3932160 | tf_op jit(solution)/shard_map/reduce_scatter | solution.py:56
  34.2 84.5 %copy-start.4 = (bf16[640,2048]{1,0:T(8,128)(2,1)S(1)}, bf16[640,2048]{1,0:T(8,128)(2,1)}, u32[]{:S(2)}) copy-start(bf16[640,2048]{1,0:T(8,128)(2,1)} %all-gather.13.cloned.1.call-done) | copy-start | bytes 7864324
  36.9 267.8 %copy-start.20 = (f32[1408]{0:T(1024)S(1)}, f32[1408]{0:T(1024)}, u32[]{:S(2)}) copy-start(f32[1408]{0:T(1024)} %param.28) | copy-start | bytes 16900
  320.0 8.7 %copy-start.2 = (bf16[640,1024]{1,0:T(8,128)(2,1)S(1)}, bf16[640,1024]{1,0:T(8,128)(2,1)}, u32[]{:S(2)}) copy-start(bf16[640,1024]{1,0:T(8,128)(2,1)} %param.20) | copy-start | bytes 3932164
  320.1 61.1 %all-gather.29.cloned.1.call-start = ((), (), s32[]{:S(2)}) async-start(), calls=%async_computation.14 | async-start | bytes 2359296 | tf_op jit(solution)/shard_map/all_gather | solution.py:107
  321.8 9.9 %copy-start.9 = (f32[256,512]{1,0:T(8,128)S(1)}, f32[256,512]{1,0:T(8,128)}, u32[]{:S(2)}) copy-start(f32[256,512]{1,0:T(8,128)} %param.31) | copy-start | bytes 1572868
  321.8 10.7 %copy-start.10 = (f32[256,512]{1,0:T(8,128)S(1)}, f32[256,512]{1,0:T(8,128)}, u32[]{:S(2)}) copy-start(f32[256,512]{1,0:T(8,128)} %param.30) | copy-start | bytes 1572868
  321.9 70.7 %all-gather.21.cloned.1.call-start = ((), (), s32[]{:S(2)}) async-start(), calls=%async_computation.8 | async-start | bytes 3932160 | tf_op jit(solution)/shard_map/all_gather | solution.py:50
  331.6 113.4 %all-gather.25.cloned.1.call-start = ((), (), s32[]{:S(2)}) async-start(), calls=%async_computation.10 | async-start | bytes 2359296 | tf_op jit(solution)/shard_map/all_gather | solution.py:84
  332.5 162.3 %all-gather.23.cloned.1.call-start = ((), (), s32[]{:S(2)}) async-start(), calls=%async_computation.9 | async-start | bytes 2359296 | tf_op jit(solution)/shard_map/all_gather | solution.py:83
  333.3 178.3 %reduce-scatter.6.cloned.1.call-start = ((), (), s32[]{:S(2)}) async-start(), calls=%async_computation.11 | async-start | bytes 3932160 | tf_op jit(solution)/shard_map/reduce_scatter | solution.py:56
  381.1 63.9 %copy-start.18 = (f32[2048]{0:T(1024)S(1)}, f32[2048]{0:T(1024)}, u32[]{:S(2)}) copy-start(f32[2048]{0:T(1024)} %param.22) | copy-start | bytes 24580
  381.2 63.9 %copy-start.22 = (f32[512]{0:T(512)S(1)}, f32[512]{0:T(512)}, u32[]{:S(2)}) copy-start(f32[512]{0:T(512)} %param.33) | copy-start | bytes 6148
  392.6 52.4 %copy-start.3 = (bf16[640,2048]{1,0:T(8,128)(2,1)S(1)}, bf16[640,2048]{1,0:T(8,128)(2,1)}, u32[]{:S(2)}) copy-start(bf16[640,2048]{1,0:T(8,128)(2,1)} %all-gather.21.cloned.1.call-done) | copy-start | bytes 7864324
  395.1 57.2 %copy-start.13 = (f32[512]{0:T(512)S(1)}, f32[512]{0:T(512)}, u32[]{:S(2)}) copy-start(f32[512]{0:T(512)} %param.35) | copy-start | bytes 6148
  395.1 57.2 %copy-start.14 = (f32[512]{0:T(512)S(1)}, f32[512]{0:T(512)}, u32[]{:S(2)}) copy-start(f32[512]{0:T(512)} %param.34) | copy-start | bytes 6148
  449.7 4.4 copy-start.11
  449.7 4.5 copy-start.12
  454.1 40.7 %copy-start.23 = (f32[512]{0:T(512)S(1)}, f32[512]{0:T(512)}, u32[]{:S(2)}) copy-start(f32[512]{0:T(512)} %param.32) | copy-start | bytes 6148
  502.5 9.0 %copy-start = (bf16[640,1024]{1,0:T(8,128)(2,1)S(1)}, bf16[640,1024]{1,0:T(8,128)(2,1)}, u32[]{:S(2)}) copy-start(bf16[640,1024]{1,0:T(8,128)(2,1)} %add_convert_fusion.2) | copy-start | bytes 3932164
  502.6 24.7 %all-gather.27.cloned.1.call-start = ((), (), s32[]{:S(2)}) async-start(), calls=%async_computation.12 | async-start | bytes 3932160 | tf_op jit(solution)/shard_map/all_gather | solution.py:50
  514.5 15.3 %copy-start.21 = (f32[2048]{0:T(1024)S(1)}, f32[2048]{0:T(1024)}, u32[]{:S(2)}) copy-start(f32[2048]{0:T(1024)} %param.23) | copy-start | bytes 24580
  514.5 51.0 %reduce-scatter.8.cloned.1.call-start = ((), (), s32[]{:S(2)}) async-start(), calls=%async_computation.13 | async-start | bytes 3932160 | tf_op jit(solution)/shard_map/reduce_scatter | solution.py:56
  553.8 11.6 %copy-start.1 = (bf16[640,1024]{1,0:T(8,128)(2,1)S(1)}, bf16[640,1024]{1,0:T(8,128)(2,1)}, u32[]{:S(2)}) copy-start(bf16[640,1024]{1,0:T(8,128)(2,1)} %add_convert_fusion.1) | copy-start | bytes 3932164
  (4 other events, 7.4 us)
Sparse Core Ops, SparseCore 0:
  8.9 14.0 all-gather.12
  25.2 93.4 all-gather.14
  120.9 90.4 all-gather.16
  213.3 91.2 all-gather.18
  320.2 8.4 reduce-scatter.3
  330.7 50.4 all-gather.28
  382.7 9.8 all-gather.20
  394.7 50.2 all-gather.24
  447.2 47.6 all-gather.22
  502.7 8.8 reduce-scatter.5
  514.6 12.5 all-gather.26
  554.0 11.4 reduce-scatter.7
